TPU v7x, 32 devices: a whole 2x2x4 slice. The times are simulated.
32 devices in a mesh: sp: 16 (over z, y, x), tp: 2 (over core).
Axes of the slice: x: 2, y: 2, z: 4, core: 2. Of those that a mesh axis runs over, the one named last changes fastest.
Arguments:
- resid: bfloat16 [2048, 2048], P('sp'), may hold values from -6 to 6
- queries: bfloat16 [2048, 1024], P('sp', 'tp'), may hold values from -6 to 6
- keys: bfloat16 [2048, 1024], P('sp', 'tp'), may hold values from -6 to 6
- values: bfloat16 [2048, 2048], P('sp', 'tp'), may hold values from -6 to 6
- decay_pre: float32 [2048, 1024], P('sp', 'tp'), may hold values from -4 to 11.5
- out_gate: bfloat16 [2048, 2048], P('sp', 'tp'), may hold values from -6 to 6
- head_gain: float32 [256], replicated, may hold values from 0.1 to 1.9
- out_proj: bfloat16 [2048, 2048], P('tp'), may hold values from -0.25 to 0.25
- mix_gain: float32 [2048], replicated, may hold values from 0.1 to 1.9
- mix_shift: float32 [2048], replicated, may hold values from -3 to 3
- gate_in: bfloat16 [2048, 5632], P('sp', 'tp'), may hold values from -0.125 to 0.125
- up_in: bfloat16 [2048, 5632], P('sp', 'tp'), may hold values from -0.125 to 0.125
- down_out: bfloat16 [5632, 2048], P('tp', 'sp'), may hold values from -0.25 to 0.25
- out_gain: float32 [2048], replicated, may hold values from 0.1 to 1.9
- out_shift: float32 [2048], replicated, may hold values from -2 to 2
Outputs:
- result: bfloat16 [2048, 2048], P('sp')
All inputs are finite; a program needn't handle non-finite values.
Results may differ from a plain program's by a relative error of at most 0.02.
Values may be sent and summed in bfloat16 or wider, within the bound.
A program may use at most 128 MiB of HBM per device.

v0:
```python
import jax
import jax.numpy as jnp
from jax import lax
from jax.sharding import PartitionSpec as P

HK = 128
HV = 256
SPAN = 64
ALPHA = 2.0**0.25
LN_EPS = 1e-05
RMS_EPS = 1e-06
TAU = 16.0


def entering(array, axis, combine, identity):
    count, place = (lax.axis_size(axis), lax.axis_index(axis))
    everything = jax.tree.map(
        lambda part, kind: lax.all_gather(part.astype(kind), axis),
        array,
        (jnp.bfloat16, jnp.bfloat16),
    )
    start = jax.tree.map(
        lambda part, zero: jnp.broadcast_to(jnp.asarray(zero, part.dtype), part.shape),
        array,
        identity,
    )

    def lap(k, before):
        reached = k < place
        new = combine(
            before, jax.tree.map(lambda part, own: part[k].astype(own.dtype), everything, array)
        )
        return jax.tree.map(lambda a, b: jnp.where(reached, a, b), new, before)

    return lax.fori_loop(0, count, lap, start)


def layer_norm(inputs, gain, shift):
    center = inputs - jnp.mean(inputs, axis=-1, keepdims=True)
    spread = jnp.mean(center * center, axis=-1, keepdims=True)
    return center * lax.rsqrt(spread + LN_EPS) * gain + shift


def combine_states(earlier, later):
    return (earlier[0] * later[0], later[0][..., None] * earlier[1] + later[1])


def mix_tokens(queries, keys, values, decay_pre, out_gate, head_gain):
    tok_rows = queries.shape[0]
    local_heads = queries.shape[1] // HK
    blocks = tok_rows // SPAN
    logdecay = jax.nn.log_sigmoid(decay_pre) / TAU
    scaled_q = queries.astype(jnp.float32).reshape(blocks, SPAN, local_heads, HK) * HK ** (-0.5)
    key_block = keys.astype(jnp.float32).reshape(blocks, SPAN, local_heads, HK)
    value_block = values.astype(jnp.float32).reshape(blocks, SPAN, local_heads, HV)
    cumul = jnp.cumsum(logdecay.reshape(blocks, SPAN, local_heads, HK), axis=1)
    last = cumul[:, -1]
    key_decayed = key_block * jnp.exp(last[:, None] - cumul)
    updates = jnp.einsum(
        "nchk,nchv->nhkv", key_decayed, value_block, precision=lax.Precision.HIGHEST
    )

    def advance(running_state, inputs):
        decay_end, state_increment, current_query = inputs
        running_state = jnp.exp(decay_end)[..., None] * running_state + state_increment
        return (
            running_state,
            jnp.einsum(
                "qpy,pyr->qpr", current_query, running_state, precision=lax.Precision.HIGHEST
            ),
        )

    own_state, local_read = lax.scan(
        advance, jnp.zeros((local_heads, HK, HV), jnp.float32), (last, updates, scaled_q)
    )
    block_ends = jnp.cumsum(last, axis=0)
    own_decay = jnp.exp(block_ends[-1])
    identity = (jnp.ones_like(own_decay), jnp.zeros_like(own_state))
    _, incoming = entering((own_decay, own_state), "sp", combine_states, identity)
    carried = jnp.einsum(
        "xepj,pjw->xepw",
        scaled_q * jnp.exp(block_ends)[:, None],
        incoming,
        precision=lax.Precision.HIGHEST,
    )
    state_readout = (local_read + carried).reshape(tok_rows, local_heads, HV)
    normed = (
        state_readout
        * lax.rsqrt(jnp.mean(state_readout * state_readout, axis=-1, keepdims=True) + RMS_EPS)
        * head_gain
    )
    return (
        normed.reshape(tok_rows, local_heads * HV) * jax.nn.silu(out_gate.astype(jnp.float32))
    ).astype(jnp.bfloat16)


def hidden_by_rows(whole_rows, gate_in, up_in):
    gate = jnp.dot(
        whole_rows,
        lax.all_gather(gate_in, "sp", axis=0, tiled=True),
        preferred_element_type=jnp.float32,
    )
    upward = jnp.dot(
        whole_rows,
        lax.all_gather(up_in, "sp", axis=0, tiled=True),
        preferred_element_type=jnp.float32,
    )
    return (jax.nn.silu(gate) * upward).astype(jnp.bfloat16)


def down_by_columns(hidden, down_out):
    return jnp.dot(
        hidden,
        lax.all_gather(down_out, "sp", axis=1, tiled=True),
        preferred_element_type=jnp.float32,
    )


def body(
    resid,
    queries,
    keys,
    values,
    decay_pre,
    out_gate,
    head_gain,
    out_proj,
    mix_gain,
    mix_shift,
    gate_in,
    up_in,
    down_out,
    out_gain,
    out_shift,
):
    tp_count = lax.axis_size("tp")
    tok_rows = queries.shape[0]
    own_count = tok_rows // tp_count
    gated = mix_tokens(queries, keys, values, decay_pre, out_gate, head_gain)
    mixed = lax.psum_scatter(
        jnp.dot(gated, out_proj, preferred_element_type=jnp.float32).astype(jnp.bfloat16),
        "tp",
        scatter_dimension=0,
        tiled=True,
    ).astype(jnp.float32)
    own_resid = lax.dynamic_slice_in_dim(resid, lax.axis_index("tp") * own_count, own_count, 0)
    mid = layer_norm(ALPHA * own_resid.astype(jnp.float32) + mixed, mix_gain, mix_shift).astype(
        jnp.bfloat16
    )
    whole_rows = lax.all_gather(mid, "tp", axis=0, tiled=True)
    hidden = hidden_by_rows(whole_rows, gate_in, up_in)
    ffn = lax.psum_scatter(
        down_by_columns(hidden, down_out).astype(jnp.bfloat16),
        "tp",
        scatter_dimension=0,
        tiled=True,
    ).astype(jnp.float32)
    finished = layer_norm(ALPHA * mid.astype(jnp.float32) + 0.5 * ffn, out_gain, out_shift).astype(
        jnp.bfloat16
    )
    return lax.all_gather(finished, "tp", axis=0, tiled=True)


def solution(mesh):
    return jax.shard_map(
        body,
        mesh=mesh,
        in_specs=(
            P("sp", None),
            P("sp", "tp"),
            P("sp", "tp"),
            P("sp", "tp"),
            P("sp", "tp"),
            P("sp", "tp"),
            P(),
            P("tp", None),
            P(),
            P(),
            P("sp", "tp"),
            P("sp", "tp"),
            P("tp", "sp"),
            P(),
            P(),
        ),
        out_specs=P("sp", None),
        check_vma=False,
    )
```

profile of v0, /device:TPU:0, one launch (start us, length us, event | category | flops | bytes accessed | tf_op | source)
XLA Modules:
  0.0 625.8 jit_solution(3039727210202333603)
XLA Ops:
  6.5 1.1 fusion.12
  7.7 0.1 reshape.91
  7.8 0.1 fusion.22
  7.9 1.0 reshape.101
  8.9 1.1 reshape.94
  10.0 1.0 reshape.103
  11.0 0.1 exponential_multiply_fusion
  11.1 0.6 fusion.13
  11.8 0.1 broadcast_multiply_fusion
  11.9 1.4 while.27
  11.9 0.2 bitcast_add_fusion.2
  12.1 0.4 fusion.39
  12.6 0.2 bitcast_add_fusion.2
  12.8 0.4 fusion.39
  13.3 0.7 convert_element_type.69
  14.0 0.0 reduce-scatter.3.cloned.1.call-start
  14.2 42.6 %all_gather.25 = bf16[16,4,128]{2,1,0:T(4,128)(2,1)S(1)} all-gather(bf16[1,4,128]{2,1,0:T(4,128)(2,1)S(1)} %fusion.18), channel_id=1, replica_groups=mesh['sp'=16,'tp'=2] {'sp'}, dimensions={0}, use_global_device_ids=true | all-gather | bytes 17408 | tf_op jit(solution)/shard_map/all_gather | solution.py:18
  56.8 35.8 %all-gather.12.cloned.1.call-done = bf16[64,128,256]{2,1,0:T(8,128)(2,1)} async-done(((bf16[4,128,256]{2,1,0:T(8,128)(2,1)}), bf16[64,128,256]{2,1,0:T(8,128)(2,1)}) %all-gather.12.cloned.1.call-update) | async-done | bytes 4194320 | tf_op jit(solution)/shard_map/all_gather | solution.py:18
  92.5 19.1 %while.28 = (s32[]{:T(128)}, f32[4,128,256]{2,1,0:T(8,128)S(1)}, s32[]{:T(128)}, bf16[16,4,128]{2,1,0:T(4,128)(2,1)S(1)}, bf16[16,4,128,256]{3,2,1,0:T(8,128)(2,1)}, /*index=5*/s32[]{:T(128)}, s32[]{:T(128)}) while((s32[]{:T(128)}, f32[4,128,256]{2,1,0:T(8,128)S(1)}, s32[]{:T(128)}, bf16[16,4,128]{2,1,0:T(4,128)(2,1)S(1)}, ...), condition=%wide.region_5.6_spmd.clone, body=%wide.region_4.5_spmd.clone.sunk | while | flops 655876 | bytes 1315945 | solution.py:35
  92.5 1.1 fusion.40
  93.7 1.2 fusion.40
  94.9 1.2 fusion.40
  96.1 1.2 fusion.40
  97.3 1.2 fusion.40
  98.5 1.2 fusion.40
  99.7 1.2 fusion.40
  100.9 1.2 fusion.40
  102.1 1.2 fusion.40
  103.3 1.2 fusion.40
  104.5 1.2 fusion.40
  105.7 1.2 fusion.40
  106.9 1.2 fusion.40
  108.1 1.2 fusion.40
  109.3 1.2 fusion.40
  110.5 1.2 fusion.40
  111.6 0.6 fusion.23
  112.3 0.2 multiply_reduce_fusion.2
  112.4 0.1 copy.33
  112.5 0.2 mul.156
  112.8 0.1 copy.45
  112.9 0.3 copy.31
  113.2 0.1 copy.44
  113.4 3.8 convolution_convert_fusion.1
  117.2 0.0 all-gather.6.cloned.1.call-start
  117.3 0.7 all-gather.6.cloned.1.call-update
  118.0 0.5 all-gather.10.cloned.1.call-update
  118.6 0.5 all-gather.8.cloned.1.call-update
  119.1 0.0 reduce-scatter.5.cloned.1.call-start
  119.2 4.7 reduce-scatter.3.cloned.1.call-done
  123.9 1.1 fusion.8
  125.0 1.2 multiply_reduce_fusion.1
  126.3 1.1 add_convert_fusion.1
  127.4 2.2 all_gather.28
  129.6 139.6 %all-gather.6.cloned.1.call-done = bf16[2048,2816]{1,0:T(8,128)(2,1)} async-done(((bf16[128,2816]{1,0:T(8,128)(2,1)}), bf16[2048,2816]{1,0:T(8,128)(2,1)}) %all-gather.6.cloned.1.call-update) | async-done | bytes 11534352 | tf_op jit(solution)/shard_map/all_gather | solution.py:100
  269.2 6.0 fusion.24
  275.2 176.8 %all-gather.10.cloned.1.call-done = bf16[2816,2048]{1,0:T(8,128)(2,1)} async-done(((bf16[2816,128]{1,0:T(8,128)(2,1)}), bf16[2816,2048]{1,0:T(8,128)(2,1)}) %all-gather.10.cloned.1.call-update) | async-done | bytes 11534352 | tf_op jit(solution)/shard_map/all_gather | solution.py:114
  452.0 142.2 %all-gather.8.cloned.1.call-done = bf16[2048,2816]{1,0:T(8,128)(2,1)} async-done(((bf16[128,2816]{1,0:T(8,128)(2,1)}), bf16[2048,2816]{1,0:T(8,128)(2,1)}) %all-gather.8.cloned.1.call-update) | async-done | bytes 11534352 | tf_op jit(solution)/shard_map/all_gather | solution.py:105
  594.3 11.9 %convolution_convert_fusion = bf16[128,2048]{1,0:T(8,128)(2,1)} fusion(bf16[2816,2048]{1,0:T(8,128)(2,1)} %all-gather.10.cloned.1.call-done, bf16[128,2048]{1,0:T(8,128)(2,1)S(1)} %all_gather.28, bf16[2048,2816]{1,0:T(8,128)(2,1)} %all-gather.8.cloned.1.call-done, f32[128,2816]{1,0:T(8,128)S(1)} %fusion.24), kind=kOutput, calls=%fused_computation.12 | convolution fusion | flops 2955214848 | bytes 25559040 | tf_op jit(solution)/shard_map/dot_general | solution.py:112
  606.2 6.3 %reduce-scatter.5.cloned.1.call-done = bf16[64,2048]{1,0:T(8,128)(2,1)} async-done(((bf16[128,2048]{1,0:T(8,128)(2,1)}), bf16[64,2048]{1,0:T(8,128)(2,1)}) %reduce-scatter.5.cloned.1.call-update) | async-done | bytes 262160 | tf_op jit(solution)/shard_map/reduce_scatter | solution.py:152
  612.4 1.2 fusion.9
  613.6 1.2 multiply_reduce_fusion
  614.8 1.1 add_convert_fusion
  616.0 2.2 all_gather.32
  618.2 0.8 copy.72
  (54 shorter events, 0.4 us)
Async XLA Ops:
  6.5 7.6 %copy-start = (f32[256]{0:T(256)S(1)}, f32[256]{0:T(256)}, u32[]{:S(2)}) copy-start(f32[256]{0:T(256)} %param.25) | copy-start | bytes 3076
  6.5 86.0 %all-gather.12.cloned.1.call-start = ((), (), s32[]{:S(2)}) async-start(), calls=%async_computation.7 | async-start | bytes 4456448 | tf_op jit(solution)/shard_map/all_gather | solution.py:18
  14.0 109.9 %reduce-scatter.3.cloned.1.call-start = ((), (), s32[]{:S(2)}) async-start(), calls=%async_computation.2 | async-start | bytes 786432 | tf_op jit(solution)/shard_map/reduce_scatter | solution.py:140
  111.6 1.7 copy-start.6
  113.3 10.6 %copy-start.1 = (bf16[128,2048]{1,0:T(8,128)(2,1)S(1)}, bf16[128,2048]{1,0:T(8,128)(2,1)}, u32[]{:S(2)}) copy-start(bf16[128,2048]{1,0:T(8,128)(2,1)} %param.19) | copy-start | bytes 1572868
  113.3 12.9 %copy-start.2 = (f32[2048]{0:T(1024)S(1)}, f32[2048]{0:T(1024)}, u32[]{:S(2)}) copy-start(f32[2048]{0:T(1024)} %param.28) | copy-start | bytes 24580
  113.3 12.9 %copy-start.3 = (f32[2048]{0:T(1024)S(1)}, f32[2048]{0:T(1024)}, u32[]{:S(2)}) copy-start(f32[2048]{0:T(1024)} %param.27) | copy-start | bytes 24580
  117.2 152.0 %all-gather.6.cloned.1.call-start = ((), (), s32[]{:S(2)}) async-start(), calls=%async_computation.3 | async-start | bytes 12255232 | tf_op jit(solution)/shard_map/all_gather | solution.py:100
  118.0 334.1 %all-gather.10.cloned.1.call-start = ((), (), s32[]{:S(2)}) async-start(), calls=%async_computation.5 | async-start | bytes 12255232 | tf_op jit(solution)/shard_map/all_gather | solution.py:114
  118.5 475.7 %all-gather.8.cloned.1.call-start = ((), (), s32[]{:S(2)}) async-start(), calls=%async_computation.4 | async-start | bytes 12255232 | tf_op jit(solution)/shard_map/all_gather | solution.py:105
  119.1 493.3 %reduce-scatter.5.cloned.1.call-start = ((), (), s32[]{:S(2)}) async-start(), calls=%async_computation.6 | async-start | bytes 786432 | tf_op jit(solution)/shard_map/reduce_scatter | solution.py:152
  275.2 339.6 %copy-start.4 = (f32[2048]{0:T(1024)S(1)}, f32[2048]{0:T(1024)}, u32[]{:S(2)}) copy-start(f32[2048]{0:T(1024)} %param.33) | copy-start | bytes 24580
  275.2 339.6 %copy-start.5 = (f32[2048]{0:T(1024)S(1)}, f32[2048]{0:T(1024)}, u32[]{:S(2)}) copy-start(f32[2048]{0:T(1024)} %param.32) | copy-start | bytes 24580
Sparse Core Ops, SparseCore 0:
  14.1 78.3 all-gather.11
  117.3 6.5 reduce-scatter.2
  126.7 142.5 all-gather.5
  271.8 180.2 all-gather.9
  454.6 139.5 all-gather.7
  606.3 6.0 reduce-scatter.4
where the time goes:
time: 627 us; the launch traced here: 626 us
  waiting for transfers between devices  507 us (81%)
  blocking collectives  47 us (7%)
  other arithmetic  28.2 us (4%)
  matrix products  23.8 us (4%)
  between operations  13.8 us (2%)
    all_gather x1, waiting for transfers between devices, down_by_columns(): lax.all_gather(down_out, 'sp', axis=1, tiled=True)  177 us
    all_gather x1, waiting for transfers between devices, hidden_by_rows(): lax.all_gather(up_in, 'sp', axis=0, tiled=True)  142 us
    all_gather x1, waiting for transfers between devices, hidden_by_rows(): lax.all_gather(gate_in, 'sp', axis=0, tiled=True)  140 us
    all_gather x1, blocking collectives, entering(): lax.all_gather(part.astype(kind), axis)  42.6 us
    all_gather x1, waiting for transfers between devices, entering(): lax.all_gather(part.astype(kind), axis)  35.8 us
    select_n x16, other arithmetic, lap(): return jax.tree.map(lambda a, b: jnp.where(reached, a, b), new, before)  18.4 us
  transfers between devices with their start and end apart: 6, of which 6 were waited for; matrix products, arithmetic and copies ran while one was open for 2% of the time, Pallas kernels for 0%

commit v1 on v0

--- a/solution.py
+++ b/solution.py
@@ -111,7 +111,7 @@
 def down_by_columns(hidden, down_out):
     return jnp.dot(
         hidden,
-        lax.all_gather(down_out, "sp", axis=1, tiled=True),
+        jnp.concatenate(lax.all_gather(down_out, "sp"), axis=1),
         preferred_element_type=jnp.float32,
     )
 

time: 627 us -> 588 us (0.938)
  waiting for transfers between devices: 507 us -> 451 us
  local copies, waits for them, and re-layouts: 4.97 us -> 20.2 us
    all_gather x1, waiting for transfers between devices: 177 us -> 139 us  [down_by_columns(): lax.all_gather(down_out, 'sp')]
    reshape x0 -> x1, local copies, waits for them, and re-layouts: none -> 15.2 us  [down_by_columns(): jnp.concatenate(lax.all_gather(down_out, 'sp'), axis=1)]
    all_gather x1, waiting for transfers between devices: 140 us -> 127 us  [hidden_by_rows(): lax.all_gather(gate_in, 'sp', axis=0, tiled=True)]
  transfers between devices with their start and end apart: 6 -> 6, of which waited for: 6 -> 6; matrix products, arithmetic and copies ran while one was open for 2% -> 4% of each run, Pallas kernels for 0% -> 0%
where the time goes in v1:
time: 588 us; the launch traced here: 587 us
  waiting for transfers between devices  451 us (77%)
  blocking collectives  47.1 us (8%)
  other arithmetic  28.2 us (5%)
  matrix products  25.2 us (4%)
  local copies, waits for them, and re-layouts  20.2 us (3%)
  between operations  13.8 us (2%)
    all_gather x1, waiting for transfers between devices, down_by_columns(): lax.all_gather(down_out, 'sp')  139 us
    all_gather x1, waiting for transfers between devices, hidden_by_rows(): lax.all_gather(up_in, 'sp', axis=0, tiled=True)  136 us
    all_gather x1, waiting for transfers between devices, hidden_by_rows(): lax.all_gather(gate_in, 'sp', axis=0, tiled=True)  127 us
    all_gather x1, blocking collectives, entering(): lax.all_gather(part.astype(kind), axis)  42.6 us
    all_gather x1, waiting for transfers between devices, entering(): lax.all_gather(part.astype(kind), axis)  35.8 us
    select_n x16, other arithmetic, lap(): return jax.tree.map(lambda a, b: jnp.where(reached, a, b), new, before)  18.4 us
    reshape x1, local copies, waits for them, and re-layouts, down_by_columns(): jnp.concatenate(lax.all_gather(down_out, 'sp'), axis=1)  15.2 us
    dot_general x1, matrix products, down_by_columns(): jnp.dot(hidden, jnp.concatenate(lax.all_gather(down_out, 'sp'), axis=1),...  13.3 us
  transfers between devices with their start and end apart: 6, of which 6 were waited for; matrix products, arithmetic and copies ran while one was open for 4% of the time, Pallas kernels for 0%

profile of v1, /device:TPU:0, one launch (start us, length us, event | category | flops | bytes accessed | tf_op | source)
XLA Modules:
  0.0 586.6 jit_solution(4975677808484829431)
XLA Ops:
  6.5 1.1 fusion.12
  7.7 0.1 reshape.97
  7.8 0.1 fusion.22
  7.9 1.0 reshape.109
  8.9 1.1 reshape.100
  10.0 1.0 reshape.111
  11.0 0.1 exponential_multiply_fusion
  11.1 0.6 fusion.13
  11.8 0.1 broadcast_multiply_fusion
  11.9 1.4 while.27
  11.9 0.2 bitcast_add_fusion.2
  12.1 0.4 fusion.39
  12.6 0.2 bitcast_add_fusion.2
  12.8 0.4 fusion.39
  13.3 0.7 convert_element_type.69
  14.0 0.0 reduce-scatter.3.cloned.1.call-start
  14.2 42.6 %all_gather.28 = bf16[16,4,128]{2,1,0:T(4,128)(2,1)S(1)} all-gather(bf16[1,4,128]{2,1,0:T(4,128)(2,1)S(1)} %fusion.18), channel_id=1, replica_groups=mesh['sp'=16,'tp'=2] {'sp'}, dimensions={0}, use_global_device_ids=true | all-gather | bytes 17408 | tf_op jit(solution)/shard_map/all_gather | solution.py:18
  56.8 35.8 %all-gather.11.cloned.1.call-done = bf16[64,128,256]{2,1,0:T(8,128)(2,1)} async-done(((bf16[4,128,256]{2,1,0:T(8,128)(2,1)}), bf16[64,128,256]{2,1,0:T(8,128)(2,1)}) %all-gather.11.cloned.1.call-update) | async-done | bytes 4194320 | tf_op jit(solution)/shard_map/all_gather | solution.py:18
  92.5 19.1 %while.28 = (s32[]{:T(128)}, f32[4,128,256]{2,1,0:T(8,128)S(1)}, s32[]{:T(128)}, bf16[16,4,128]{2,1,0:T(4,128)(2,1)S(1)}, bf16[16,4,128,256]{3,2,1,0:T(8,128)(2,1)}, /*index=5*/s32[]{:T(128)}, s32[]{:T(128)}) while((s32[]{:T(128)}, f32[4,128,256]{2,1,0:T(8,128)S(1)}, s32[]{:T(128)}, bf16[16,4,128]{2,1,0:T(4,128)(2,1)S(1)}, ...), condition=%wide.region_5.6_spmd.clone, body=%wide.region_4.5_spmd.clone.sunk | while | flops 655876 | bytes 1315945 | solution.py:35
  92.5 1.1 fusion.40
  93.7 1.2 fusion.40
  94.9 1.2 fusion.40
  96.1 1.2 fusion.40
  97.3 1.2 fusion.40
  98.5 1.2 fusion.40
  99.7 1.2 fusion.40
  100.9 1.2 fusion.40
  102.1 1.2 fusion.40
  103.3 1.2 fusion.40
  104.5 1.2 fusion.40
  105.7 1.2 fusion.40
  106.9 1.2 fusion.40
  108.1 1.2 fusion.40
  109.3 1.2 fusion.40
  110.5 1.2 fusion.40
  111.6 0.6 fusion.23
  112.3 0.2 multiply_reduce_fusion.2
  112.4 0.1 copy.41
  112.5 0.2 mul.156
  112.8 0.1 copy.53
  112.9 0.3 copy.38
  113.2 0.1 copy.52
  113.4 3.8 convolution_convert_fusion.1
  117.2 0.0 all-gather.13.cloned.1.call-start
  117.3 0.7 all-gather.13.cloned.1.call-update
  118.0 0.5 all-gather.7.cloned.1.call-update
  118.6 0.5 all-gather.9.cloned.1.call-update
  119.2 4.7 reduce-scatter.3.cloned.1.call-done
  123.9 1.1 fusion.8
  125.1 1.2 multiply_reduce_fusion.1
  126.3 1.1 add_convert_fusion.1
  127.4 2.4 all_gather.31
  129.8 139.5 %all-gather.13.cloned.1.call-done = bf16[45056,128]{1,0:T(8,128)(2,1)} async-done(((bf16[2816,128]{1,0:T(8,128)(2,1)}), bf16[45056,128]{1,0:T(8,128)(2,1)}) %all-gather.13.cloned.1.call-update) | async-done | bytes 11534352 | tf_op jit(solution)/shard_map/all_gather | solution.py:114
  269.2 15.2 %copy.40 = bf16[2816,16,128]{0,2,1:T(8,128)(2,1)} copy(bf16[2816,16,128]{2,0,1:T(8,128)(2,1)} %bitcast.70) | data formatting | bytes 23068672 | tf_op jit(solution)/shard_map/reshape | solution.py:114
  284.4 127.1 %all-gather.7.cloned.1.call-done = bf16[2048,2816]{1,0:T(8,128)(2,1)} async-done(((bf16[128,2816]{1,0:T(8,128)(2,1)}), bf16[2048,2816]{1,0:T(8,128)(2,1)}) %all-gather.7.cloned.1.call-update) | async-done | bytes 11534352 | tf_op jit(solution)/shard_map/all_gather | solution.py:100
  411.5 6.0 %fusion.24 = f32[128,2816]{1,0:T(8,128)S(1)} fusion(bf16[128,2048]{1,0:T(8,128)(2,1)S(1)} %all_gather.31, bf16[2048,2816]{1,0:T(8,128)(2,1)} %all-gather.7.cloned.1.call-done), kind=kOutput, calls=%fused_computation.56 | convolution fusion | flops 1476395008 | bytes 13500416 | tf_op jit(solution)/shard_map/dot_general | solution.py:98
  417.4 136.3 %all-gather.9.cloned.1.call-done = bf16[2048,2816]{1,0:T(8,128)(2,1)} async-done(((bf16[128,2816]{1,0:T(8,128)(2,1)}), bf16[2048,2816]{1,0:T(8,128)(2,1)}) %all-gather.9.cloned.1.call-update) | async-done | bytes 11534352 | tf_op jit(solution)/shard_map/all_gather | solution.py:105
  553.7 13.3 %convolution_convert_fusion = bf16[128,2048]{1,0:T(8,128)(2,1)} fusion(bf16[2816,2048]{0,1:T(8,128)(2,1)} %bitcast.71, bf16[128,2048]{1,0:T(8,128)(2,1)S(1)} %all_gather.31, bf16[2048,2816]{1,0:T(8,128)(2,1)} %all-gather.9.cloned.1.call-done, f32[128,2816]{1,0:T(8,128)S(1)} %fusion.24), kind=kOutput, calls=%fused_computation.12 | convolution fusion | flops 2955214848 | bytes 25559040 | tf_op jit(solution)/shard_map/dot_general | solution.py:112
  567.0 6.3 %reduce-scatter.5.cloned.1.call-done = bf16[64,2048]{1,0:T(8,128)(2,1)} async-done(((bf16[128,2048]{1,0:T(8,128)(2,1)}), bf16[64,2048]{1,0:T(8,128)(2,1)}) %reduce-scatter.5.cloned.1.call-update) | async-done | bytes 262160 | tf_op jit(solution)/shard_map/reduce_scatter | solution.py:152
  573.3 1.2 fusion.9
  574.4 1.2 multiply_reduce_fusion
  575.7 1.1 add_convert_fusion
  576.8 2.2 all_gather.36
  579.0 0.8 copy.80
  (57 shorter events, 0.5 us)
Async XLA Ops:
  6.5 7.6 %copy-start = (f32[256]{0:T(256)S(1)}, f32[256]{0:T(256)}, u32[]{:S(2)}) copy-start(f32[256]{0:T(256)} %param.25) | copy-start | bytes 3076
  6.5 86.0 %all-gather.11.cloned.1.call-start = ((), (), s32[]{:S(2)}) async-start(), calls=%async_computation.6 | async-start | bytes 4456448 | tf_op jit(solution)/shard_map/all_gather | solution.py:18
  14.0 109.9 %reduce-scatter.3.cloned.1.call-start = ((), (), s32[]{:S(2)}) async-start(), calls=%async_computation.2 | async-start | bytes 786432 | tf_op jit(solution)/shard_map/reduce_scatter | solution.py:140
  111.6 1.7 copy-start.7
  113.3 10.6 %copy-start.2 = (bf16[128,2048]{1,0:T(8,128)(2,1)S(1)}, bf16[128,2048]{1,0:T(8,128)(2,1)}, u32[]{:S(2)}) copy-start(bf16[128,2048]{1,0:T(8,128)(2,1)} %param.19) | copy-start | bytes 1572868
  113.3 12.9 %copy-start.3 = (f32[2048]{0:T(1024)S(1)}, f32[2048]{0:T(1024)}, u32[]{:S(2)}) copy-start(f32[2048]{0:T(1024)} %param.28) | copy-start | bytes 24580
  113.3 12.9 %copy-start.4 = (f32[2048]{0:T(1024)S(1)}, f32[2048]{0:T(1024)}, u32[]{:S(2)}) copy-start(f32[2048]{0:T(1024)} %param.27) | copy-start | bytes 24580
  117.2 152.0 %all-gather.13.cloned.1.call-start = ((), (), s32[]{:S(2)}) async-start(), calls=%async_computation.7 | async-start | bytes 12255232 | tf_op jit(solution)/shard_map/all_gather | solution.py:114
  118.0 293.5 %all-gather.7.cloned.1.call-start = ((), (), s32[]{:S(2)}) async-start(), calls=%async_computation.3 | async-start | bytes 12255232 | tf_op jit(solution)/shard_map/all_gather | solution.py:100
  118.5 435.2 %all-gather.9.cloned.1.call-start = ((), (), s32[]{:S(2)}) async-start(), calls=%async_computation.4 | async-start | bytes 12255232 | tf_op jit(solution)/shard_map/all_gather | solution.py:105
  119.1 454.1 %reduce-scatter.5.cloned.1.call-start = ((), (), s32[]{:S(2)}) async-start(), calls=%async_computation.5 | async-start | bytes 786432 | tf_op jit(solution)/shard_map/reduce_scatter | solution.py:152
  553.7 21.9 %copy-start.5 = (f32[2048]{0:T(1024)S(1)}, f32[2048]{0:T(1024)}, u32[]{:S(2)}) copy-start(f32[2048]{0:T(1024)} %param.33) | copy-start | bytes 24580
  553.7 21.9 %copy-start.6 = (f32[2048]{0:T(1024)S(1)}, f32[2048]{0:T(1024)}, u32[]{:S(2)}) copy-start(f32[2048]{0:T(1024)} %param.32) | copy-start | bytes 24580
  553.7 26.1 %copy-start.1 = (f32[256]{0:T(256)S(1)}, f32[256]{0:T(256)}, u32[]{:S(2)}) copy-start(f32[256]{0:T(256)} %param.25) | copy-start | bytes 3076
Sparse Core Ops, SparseCore 0:
  14.1 78.3 all-gather.10
  117.3 6.5 reduce-scatter.2
  126.7 142.5 all-gather.12
  271.8 139.5 all-gather.6
  414.1 139.5 all-gather.8
  567.1 6.0 reduce-scatter.4
